TPU v7x, 32 devices: a whole 2x2x4 slice. The times are simulated.
32 devices in a mesh: sp: 8 (over z, y), tp: 4 (over x, core).
Axes of the slice: x: 2, y: 2, z: 4, core: 2. Of those that a mesh axis runs over, the one named last changes fastest.
Arguments:
- tokens: bfloat16 [8192, 2048], P('sp'), may hold values from -6 to 6
- norm_gain: float32 [2048], replicated, may hold values from 0.1 to 1.9
- w_query: bfloat16 [2048, 1024], P('sp', 'tp'), may hold values from -3.5 to 3.5
- w_key: bfloat16 [2048, 256], P('sp', 'tp'), may hold values from -0.125 to 0.125
- w_value: bfloat16 [2048, 256], P('sp', 'tp'), may hold values from -0.125 to 0.125
- w_content: bfloat16 [2048, 1024], P('sp', 'tp'), may hold values from -0.125 to 0.125
- w_gate: bfloat16 [2048, 1024], P('sp', 'tp'), may hold values from -0.125 to 0.125
- sink_logit: float32 [16], P('tp'), may hold values from 1 to 6
- conv_weight: float32 [31, 1024], P(None, 'tp'), may hold values from -10 to 10
- conv_bias: float32 [1024], P('tp'), may hold values from 0 to 20
- channel_gain: float32 [1024], P('tp'), may hold values from 0.1 to 1.9
- out_attn: bfloat16 [1024, 2048], P('tp', 'sp'), may hold values from -0.75 to 0.75
- out_conv: bfloat16 [1024, 2048], P('tp', 'sp'), may hold values from -0.1875 to 0.1875
Outputs:
- mixed: bfloat16 [8192, 2048], P(('sp', 'tp'))
All inputs are finite; a program needn't handle non-finite values.
Results may differ from a plain program's by a relative error of at most 0.025.
The roundings to bfloat16 on the way count: a program that leaves them out, or rounds other values in their place, can miss the bound.
Values may be sent and summed in bfloat16 or wider, within the bound.
A program may use at most 64 MiB of HBM per device.

v0:
```python
import math
import jax
import jax.numpy as jnp
from jax import lax
from jax.sharding import PartitionSpec as P

HEAD_DIM = 64
CONV_CH = 1024
KERNEL = 31
WINDOW = 128
EPS = 1e-05
THETA = 10000.0


def shifted(block, axis, distance):
    devices = range(lax.axis_size(axis))
    route = [(i - distance, i) for i in devices if i - distance in devices]
    return lax.ppermute(block, axis, route)


def rotate(heads_in, positions):
    half_dim = heads_in.shape[-1] // 2
    inverse = 1.0 / THETA ** (jnp.arange(half_dim, dtype=jnp.float32) * 2.0 / heads_in.shape[-1])
    angles = positions.astype(jnp.float32)[:, None] * inverse[None, :]
    cosine = jnp.cos(angles)[:, None, :]
    sine_part = jnp.sin(angles)[:, None, :]
    former = heads_in[..., :half_dim]
    latter = heads_in[..., half_dim:]
    return jnp.concatenate(
        [former * cosine - latter * sine_part, latter * cosine + former * sine_part], axis=-1
    )


def shards(
    tokens,
    norm_gain,
    w_query,
    w_key,
    w_value,
    w_content,
    w_gate,
    sink_logit,
    conv_weight,
    conv_bias,
    channel_gain,
    out_attn,
    out_conv,
):
    token_count = tokens.shape[0]
    offset = lax.axis_index("sp") * token_count
    positions = offset + jnp.arange(token_count, dtype=jnp.int32)
    tokens_wide = tokens.astype(jnp.float32)
    inv_rms = lax.rsqrt(jnp.mean(tokens_wide * tokens_wide, axis=1, keepdims=True) + EPS)
    scaled = (tokens_wide * norm_gain[None, :]).astype(jnp.bfloat16)
    widths = [
        w_query.shape[1],
        w_key.shape[1],
        w_value.shape[1],
        w_content.shape[1],
        w_gate.shape[1],
    ]
    whole_weights = (
        lax.all_gather(w_query, "sp", axis=0, tiled=True),
        lax.all_gather(w_key, "sp", axis=0, tiled=True),
        lax.all_gather(w_value, "sp", axis=0, tiled=True),
        lax.all_gather(w_content, "sp", axis=0, tiled=True),
        lax.all_gather(w_gate, "sp", axis=0, tiled=True),
    )
    joined_whole = jnp.concatenate(whole_weights, axis=1)
    projected = jnp.dot(scaled, joined_whole, preferred_element_type=jnp.float32)
    projected = projected * inv_rms
    bounds = [0]
    for width in widths:
        bounds.append(bounds[-1] + width)
    proj_query = projected[:, bounds[0] : bounds[1]]
    proj_key = projected[:, bounds[1] : bounds[2]]
    proj_value = projected[:, bounds[2] : bounds[3]]
    proj_content = projected[:, bounds[3] : bounds[4]]
    proj_gate = projected[:, bounds[4] : bounds[5]]
    kv_local = widths[1] // HEAD_DIM
    heads_local = widths[0] // HEAD_DIM
    group_size = heads_local // kv_local
    queries = rotate(proj_query.reshape(token_count, heads_local, HEAD_DIM), positions).astype(
        jnp.bfloat16
    )
    key_rows = rotate(proj_key.reshape(token_count, kv_local, HEAD_DIM), positions).astype(
        jnp.bfloat16
    )
    value_rows = proj_value.astype(jnp.bfloat16).reshape(token_count, kv_local, HEAD_DIM)
    glu_out = (proj_content * jax.nn.sigmoid(proj_gate)).astype(jnp.bfloat16)
    prior_key, prior_value, prior_glu = shifted(
        (
            key_rows[token_count - WINDOW :],
            value_rows[token_count - WINDOW :],
            glu_out[token_count - (KERNEL - 1) :],
        ),
        "sp",
        1,
    )
    key_ext = jnp.concatenate([prior_key, key_rows], 0)
    value_ext = jnp.concatenate([prior_value, value_rows], 0)
    block_rows = math.gcd(token_count, 512)
    sink_col = sink_logit.reshape(kv_local, group_size)[:, :, None, None]

    def attend(block_start):
        query_blk = lax.dynamic_slice_in_dim(queries, block_start, block_rows, 0).reshape(
            block_rows, kv_local, group_size, HEAD_DIM
        )
        key_blk = lax.dynamic_slice_in_dim(key_ext, block_start, block_rows + WINDOW, 0)
        value_blk = lax.dynamic_slice_in_dim(value_ext, block_start, block_rows + WINDOW, 0)
        scores = jnp.einsum(
            "qkgd,jkd->kgqj", query_blk, key_blk, preferred_element_type=jnp.float32
        ) * HEAD_DIM ** (-0.5)
        query_pos = offset + block_start + jnp.arange(block_rows, dtype=jnp.int32)
        key_pos = offset + block_start - WINDOW + jnp.arange(block_rows + WINDOW, dtype=jnp.int32)
        distance = query_pos[:, None] - key_pos[None, :]
        allowed = (distance >= 0) & (distance < WINDOW) & (key_pos[None, :] >= 0)
        scores = jnp.where(allowed[None, None], scores, -1e30)
        row_max = jnp.maximum(jnp.max(scores, axis=-1, keepdims=True), sink_col)
        weights = jnp.exp(scores - row_max)
        denominator = jnp.sum(weights, axis=-1, keepdims=True) + jnp.exp(sink_col - row_max)
        probability = (weights / denominator).astype(jnp.bfloat16)
        attended = jnp.einsum(
            "kgqj,jkd->qkgd", probability, value_blk, preferred_element_type=jnp.float32
        )
        return attended.reshape(block_rows, heads_local * HEAD_DIM).astype(jnp.bfloat16)

    starts = jnp.arange(0, token_count, block_rows, dtype=jnp.int32)
    attn_out = lax.map(attend, starts).reshape(token_count, heads_local * HEAD_DIM)
    padded = jnp.concatenate([prior_glu, glu_out], 0)
    conv_sum = jnp.zeros(glu_out.shape, jnp.float32) + conv_bias[None, :]
    for tap_index in range(KERNEL):
        window_rows = lax.slice_in_dim(padded, tap_index, tap_index + token_count, axis=0)
        conv_sum = conv_sum + conv_weight[tap_index][None, :] * window_rows.astype(jnp.float32)
    row_sum, row_squares = lax.psum(
        (jnp.sum(conv_sum, axis=1), jnp.sum(conv_sum * conv_sum, axis=1)), "tp"
    )
    centre = row_sum / CONV_CH
    variance = jnp.maximum(row_squares / CONV_CH - centre * centre, 0.0)
    centred = conv_sum - centre[:, None]
    conv_out = jax.nn.silu(
        centred * lax.rsqrt(variance + EPS)[:, None] * channel_gain[None, :]
    ).astype(jnp.bfloat16)
    attn_weight, conv_weight_out = (
        lax.all_gather(out_attn, "sp", axis=1, tiled=True),
        lax.all_gather(out_conv, "sp", axis=1, tiled=True),
    )
    return lax.psum_scatter(
        (
            jnp.dot(attn_out, attn_weight, preferred_element_type=jnp.float32)
            + jnp.dot(conv_out, conv_weight_out, preferred_element_type=jnp.float32)
        ).astype(jnp.bfloat16),
        "tp",
        scatter_dimension=0,
        tiled=True,
    )


def solution(mesh):
    placed = (
        P("sp", None),
        P(),
        P("sp", "tp"),
        P("sp", "tp"),
        P("sp", "tp"),
        P("sp", "tp"),
        P("sp", "tp"),
        P("tp"),
        P(None, "tp"),
        P("tp"),
        P("tp"),
        P("tp", "sp"),
        P("tp", "sp"),
    )
    return jax.shard_map(
        shards, mesh=mesh, in_specs=placed, out_specs=P(("sp", "tp"), None), check_vma=False
    )
```

profile of v0, /device:TPU:0, one launch (start us, length us, event | category | flops | bytes accessed | tf_op | source)
XLA Modules:
  0.0 276.7 jit_solution(9602372100434839561)
XLA Ops:
  6.5 0.7 all-gather.6.cloned.1.call-update
  7.3 0.0 all-gather.8.cloned.1.call-start
  7.3 0.7 all-gather.8.cloned.1.call-update
  8.0 0.0 all-gather.10.cloned.1.call-start
  8.1 0.7 all-gather.10.cloned.1.call-update
  8.7 0.0 all-gather.12.cloned.1.call-start
  8.8 0.5 all-gather.12.cloned.1.call-update
  9.3 0.0 all-gather.14.cloned.1.call-start
  9.4 0.5 all-gather.14.cloned.1.call-update
  9.9 0.0 reduce-scatter.2.cloned.1.call-start
  10.0 1.0 fusion.76
  11.0 1.0 fusion.75
  12.0 3.1 %fusion.20 = f32[1024]{0:T(1024)S(1)} fusion(bf16[1024,2048]{1,0:T(8,128)(2,1)} %param.15), kind=kLoop, calls=%fused_computation.31 | loop fusion | flops 6290432 | bytes 4198400 | tf_op jit(solution)/shard_map/reduce_sum | solution.py:53
  15.1 0.0 copy-start.3
  15.1 0.9 copy.18
  16.0 0.9 copy.19
  16.9 33.8 %all_gather.23 = bf16[2048,64]{1,0:T(8,128)(2,1)S(1)} all-gather(bf16[256,64]{1,0:T(8,128)(2,1)S(1)} %copy.19), channel_id=1, replica_groups=mesh['sp'=8,'tp'=4] {'sp'}, dimensions={0}, use_global_device_ids=true | all-gather | bytes 294912 | tf_op jit(solution)/shard_map/all_gather | solution.py:65
  50.6 31.7 %all_gather.22 = bf16[2048,64]{1,0:T(8,128)(2,1)S(1)} all-gather(bf16[256,64]{1,0:T(8,128)(2,1)S(1)} %copy.18), channel_id=1, replica_groups=mesh['sp'=8,'tp'=4] {'sp'}, dimensions={0}, use_global_device_ids=true | all-gather | bytes 294912 | tf_op jit(solution)/shard_map/all_gather | solution.py:64
  82.4 0.5 multiply_cosine_fusion
  82.9 0.0 all-gather.6.cloned.1.call-done
  83.0 14.4 %all-gather.8.cloned.1.call-done = bf16[2048,256]{1,0:T(8,128)(2,1)} async-done(((bf16[256,256]{1,0:T(8,128)(2,1)}), bf16[2048,256]{1,0:T(8,128)(2,1)}) %all-gather.8.cloned.1.call-update) | async-done | bytes 1048592 | tf_op jit(solution)/shard_map/all_gather | solution.py:66
  97.4 41.2 %all-gather.10.cloned.1.call-done = bf16[2048,256]{1,0:T(8,128)(2,1)} async-done(((bf16[256,256]{1,0:T(8,128)(2,1)}), bf16[2048,256]{1,0:T(8,128)(2,1)}) %all-gather.10.cloned.1.call-update) | async-done | bytes 1048592 | tf_op jit(solution)/shard_map/all_gather | solution.py:67
  138.5 6.7 %concatenate.28 = bf16[2048,896]{1,0:T(8,128)(2,1)} concatenate(bf16[2048,256]{1,0:T(8,128)(2,1)} %all-gather.6.cloned.1.call-done, bf16[2048,64]{1,0:T(8,128)(2,1)S(1)} %all_gather.22, bf16[2048,64]{1,0:T(8,128)(2,1)S(1)} %all_gather.23, bf16[2048,256]{1,0:T(8,128)(2,1)} %all-gather.8.cloned.1.call-done, bf16[2048,256]{1,0:T(8,128)(2,1)} %all-gather.10.cloned.1.call-done), dimensions={1} | concatenate | bytes 7340032 | tf_op jit(solution)/shard_map/concatenate | solution.py:69
  145.2 7.0 %fusion.77 = (bf16[1024,896]{0,1:T(8,128)(2,1)S(1)}, f32[1024,896]{0,1:T(8,128)S(1)}) fusion(f32[1024]{0:T(1024)S(1)} %add_rsqrt_fusion.1, bf16[2048,896]{1,0:T(8,128)(2,1)} %concatenate.28, bf16[1024,2048]{1,0:T(8,128)(2,1)} %param.15, f32[2048]{0:T(1024)S(1)} %copy-done.3), kind=kOutput, calls=%fused_computation.147 | convolution fusion | flops 3766222848 | bytes 13381632 | tf_op jit(solution)/shard_map/dot_general | solution.py:70
  152.2 0.0 copy-start.1
  152.3 0.0 copy-start
  152.3 0.3 fusion.31
  152.6 2.4 collective-permute-start
  155.0 0.6 fusion.70
  155.6 3.1 %collective-permute-start.1 = (bf16[128,1,64]{0,2,1:T(8,128)(2,1)S(1)}, bf16[128,1,64]{0,2,1:T(8,128)(2,1)S(1)}, u32[]{:S(2)}, u32[]{:S(2)}) collective-permute-start(bf16[128,1,64]{0,2,1:T(8,128)(2,1)S(1)} %pad_maximum_fusion.3), channel_id=1, source_target_pairs={{0,4},{4,8},{8,12},{12,16},{16,20},{20,24},{24,28},{1,5},{5,9},{9,... | collective-permute-start | bytes 49160 | tf_op jit(solution)/shard_map/ppermute | solution.py:18
  158.7 0.1 slice.308
  158.8 2.5 collective-permute-start.2
  161.4 0.2 subtract_convert_fusion
  161.6 1.7 collective-permute-done.2
  163.3 0.0 copy-done.1
  163.3 7.8 %fusion.74 = (f32[1024]{0:T(1024)S(1)}, f32[1024]{0:T(1024)S(1)}, f32[1024,256]{0,1:T(8,128)S(1)}) fusion(bf16[1024,256]{0,1:T(8,128)(2,1)S(1)} %get-tuple-element.130, f32[256]{0:T(256)S(1)} %bitcast.115, bf16[30,256]{0,1:T(8,128)(2,1)S(1)} %collective-permute-done.2, f32[256]{0:T(256)S(1)} %bitcast.116, f32[256]{0:T(256)S(1)} %bitcast.118, ...), kind=kLoop, calls=%fused_computation.144 | loop fusion | flops 48756736 | bytes 1629184 | tf_op jit(solution)/shard_map/reduce_sum | solution.py:136
  171.1 6.1 %all-reduce = (f32[1024]{0:T(1024)S(1)}, f32[1024]{0:T(1024)S(1)}) all-reduce(f32[1024]{0:T(1024)S(1)} %get-tuple-element.108, f32[1024]{0:T(1024)S(1)} %get-tuple-element.107), channel_id=1, replica_groups=mesh['sp'=8,'tp'=4] {'tp'}, use_global_device_ids=true, to_apply=%region_8.9 | all-reduce | flops 2048 | bytes 16384 | tf_op jit(solution)/shard_map/psum | solution.py:135
  177.2 0.0 collective-permute-done.1
  177.2 0.0 collective-permute-done
  177.3 0.0 copy-done
  177.3 18.4 %while.12 = (s32[]{:T(128)}, bf16[2,512,256]{2,1,0:T(8,128)(2,1)S(1)}, s32[2]{0:T(128)S(1)}, bf16[1152,1,64]{0,2,1:T(8,128)(2,1)S(1)}, s32[]{:T(128)}, /*index=5...) while((s32[]{:T(128)}, ...), condition=%wide.region_4.5_spmd, body=%wide.region_1.4_spmd.sunk | while | flops 353048960 | bytes 18868768 | solution.py:129
  177.3 0.6 dynamic_slice.46
  181.7 0.4 fusion.91
  182.1 1.2 fusion.92
  183.4 0.1 broadcast_maximum_fusion.2
  183.4 1.1 fusion.93
  184.5 0.1 exponential_add_fusion.2
  184.6 1.7 fusion.94
  186.3 0.1 copy.25
  186.5 0.6 dynamic_slice.46
  190.9 0.4 fusion.91
  191.3 1.2 fusion.92
  192.6 0.1 broadcast_maximum_fusion.2
  192.6 1.1 fusion.93
  193.8 0.1 exponential_add_fusion.2
  193.8 1.7 fusion.94
  195.5 0.1 copy.25
  195.7 0.0 all-gather.12.cloned.1.call-done
  195.7 0.0 copy-start.2
  195.7 5.7 %fusion.78 = f32[1024,2048]{1,0:T(8,128)} fusion(bf16[1024,256]{1,0:T(8,128)(2,1)S(1)} %bitcast.101, bf16[256,2048]{1,0:T(8,128)(2,1)} %all-gather.12.cloned.1.call-done), kind=kOutput, calls=%fused_computation.148 | convolution fusion | flops 1073741824 | bytes 9961472 | tf_op jit(solution)/shard_map/dot_general | solution.py:150
  201.5 17.5 %all-gather.14.cloned.1.call-done = bf16[256,2048]{1,0:T(8,128)(2,1)} async-done(((bf16[256,256]{1,0:T(8,128)(2,1)}), bf16[256,2048]{1,0:T(8,128)(2,1)}) %all-gather.14.cloned.1.call-update) | async-done | bytes 1048592 | tf_op jit(solution)/shard_map/all_gather | solution.py:146
  218.9 7.2 %add_convert_fusion = bf16[1024,2048]{1,0:T(8,128)(2,1)} fusion(f32[1024,2048]{1,0:T(8,128)} %fusion.78, bf16[256,2048]{1,0:T(8,128)(2,1)} %all-gather.14.cloned.1.call-done, f32[1024,256]{0,1:T(8,128)S(1)} %get-tuple-element.127, f32[256]{0:T(256)S(1)} %copy-done.2, f32[1024]{0:T(1024)S(1)} %get-tuple-element.170, f32[1024]{0:T(1024)S(1)} %get-tuple-element.169), kind=kOutput, calls=%fused_computation.32 | convolution fusion | flops 1080033280 | bytes 14689280 | tf_op jit(solution)/shard_map/dot_general | solution.py:151
  226.1 0.0 reduce-scatter.2.cloned.1.call-update
  226.1 43.7 %reduce-scatter.2.cloned.1.call-done = bf16[256,2048]{1,0:T(8,128)(2,1)} async-done(((bf16[1024,2048]{1,0:T(8,128)(2,1)}), bf16[256,2048]{1,0:T(8,128)(2,1)}) %reduce-scatter.2.cloned.1.call-update) | async-done | bytes 1048592 | tf_op jit(solution)/shard_map/reduce_scatter | solution.py:148
  (24 shorter events, 0.2 us)
Async XLA Ops:
  6.5 76.4 %all-gather.6.cloned.1.call-start = ((), (), s32[]{:S(2)}) async-start(), calls=%async_computation.1 | async-start | bytes 1179648 | tf_op jit(solution)/shard_map/all_gather | solution.py:63
  7.3 90.1 %all-gather.8.cloned.1.call-start = ((), (), s32[]{:S(2)}) async-start(), calls=%async_computation.2 | async-start | bytes 1179648 | tf_op jit(solution)/shard_map/all_gather | solution.py:66
  8.0 130.5 %all-gather.10.cloned.1.call-start = ((), (), s32[]{:S(2)}) async-start(), calls=%async_computation.3 | async-start | bytes 1179648 | tf_op jit(solution)/shard_map/all_gather | solution.py:67
  8.7 187.0 %all-gather.12.cloned.1.call-start = ((), (), s32[]{:S(2)}) async-start(), calls=%async_computation.4 | async-start | bytes 1179648 | tf_op jit(solution)/shard_map/all_gather | solution.py:145
  9.3 209.6 %all-gather.14.cloned.1.call-start = ((), (), s32[]{:S(2)}) async-start(), calls=%async_computation.5 | async-start | bytes 1179648 | tf_op jit(solution)/shard_map/all_gather | solution.py:146
  9.9 260.0 %reduce-scatter.2.cloned.1.call-start = ((), (), s32[]{:S(2)}) async-start(), calls=%async_computation.6 | async-start | bytes 5242880 | tf_op jit(solution)/shard_map/reduce_scatter | solution.py:148
  15.1 130.1 %copy-start.3 = (f32[2048]{0:T(1024)S(1)}, f32[2048]{0:T(1024)}, u32[]{:S(2)}) copy-start(f32[2048]{0:T(1024)} %param.16) | copy-start | bytes 24580
  152.2 11.0 %copy-start.1 = (f32[256]{0:T(256)S(1)}, f32[256]{0:T(256)}, u32[]{:S(2)}) copy-start(f32[256]{0:T(256)} %param.24) | copy-start | bytes 3076
  152.3 25.0 %copy-start = (f32[4]{0:T(128)S(1)}, f32[4]{0:T(128)}, u32[]{:S(2)}) copy-start(f32[4]{0:T(128)} %param.22) | copy-start | bytes 52
  152.6 24.6 %collective-permute-start = (bf16[128,1,64]{0,2,1:T(8,128)(2,1)S(1)}, bf16[128,1,64]{0,2,1:T(8,128)(2,1)S(1)}, u32[]{:S(2)}, u32[]{:S(2)}) collective-permute-start(bf16[128,1,64]{0,2,1:T(8,128)(2,1)S(1)} %slice_bitcast_fusion.2), channel_id=1, source_target_pairs={{0,4},{4,8},{8,12},{12,16},{16,20},{20,24},{24,28},{1,5},{5,9},{9,... | collective-permute-start | bytes 49160 | tf_op jit(solution)/shard_map/ppermute | solution.py:18
  155.6 21.6 %collective-permute-start.1 = (bf16[128,1,64]{0,2,1:T(8,128)(2,1)S(1)}, bf16[128,1,64]{0,2,1:T(8,128)(2,1)S(1)}, u32[]{:S(2)}, u32[]{:S(2)}) collective-permute-start(bf16[128,1,64]{0,2,1:T(8,128)(2,1)S(1)} %pad_maximum_fusion.3), channel_id=1, source_target_pairs={{0,4},{4,8},{8,12},{12,16},{16,20},{20,24},{24,28},{1,5},{5,9},{9,... | collective-permute-start | bytes 49160 | tf_op jit(solution)/shard_map/ppermute | solution.py:18
  158.8 4.4 %collective-permute-start.2 = (bf16[30,256]{0,1:T(8,128)(2,1)S(1)}, bf16[30,256]{0,1:T(8,128)(2,1)S(1)}, u32[]{:S(2)}, u32[]{:S(2)}) collective-permute-start(bf16[30,256]{0,1:T(8,128)(2,1)S(1)} %slice.308), channel_id=1, source_target_pairs={{0,4},{4,8},{8,12},{12,16},{16,20},{20,24},{24,28},{1,5},{5,9},{9,... | collective-permute-start | bytes 46088 | tf_op jit(solution)/shard_map/ppermute | solution.py:18
  195.7 23.2 %copy-start.2 = (f32[256]{0:T(256)S(1)}, f32[256]{0:T(256)}, u32[]{:S(2)}) copy-start(f32[256]{0:T(256)} %param.25) | copy-start | bytes 3076
Sparse Core Ops, SparseCore 0:
  9.5 45.0 all-gather.5
  56.6 40.6 all-gather.7
  99.5 38.9 all-gather.9
  140.4 38.1 all-gather.11
  180.5 38.3 all-gather.13
  226.3 43.5 reduce-scatter.1
where the time goes:
time: 278 us; the launch traced here: 277 us
  waiting for transfers between devices  122 us (44%)
  blocking collectives  71.6 us (26%)
  matrix products  25.7 us (9%)
  other arithmetic  15.9 us (6%)
  between operations  13.7 us (5%)
  local copies, waits for them, and re-layouts  12.2 us (4%)
  starting transfers between devices  8.25 us (3%)
  loops' own time  7.56 us (3%)
    reduce_scatter x1, waiting for transfers between devices, shards(): lax.psum_scatter((jnp.dot(attn_out, attn_weight, preferred_element_type=j...  43.7 us
    all_gather x1, waiting for transfers between devices, shards(): lax.all_gather(w_gate, 'sp', axis=0, tiled=True)  41.2 us
    all_gather x1, blocking collectives, shards(): lax.all_gather(w_value, 'sp', axis=0, tiled=True)  33.8 us
    all_gather x1, blocking collectives, shards(): lax.all_gather(w_key, 'sp', axis=0, tiled=True)  31.7 us
    all_gather x1, waiting for transfers between devices, shards(): lax.all_gather(out_conv, 'sp', axis=1, tiled=True)  17.5 us
    all_gather x1, waiting for transfers between devices, shards(): lax.all_gather(w_content, 'sp', axis=0, tiled=True)  14.4 us
    ppermute x3, starting transfers between devices, shifted(): return lax.ppermute(block, axis, route)  8.06 us
    reduce_sum x1, other arithmetic, shards(): jnp.sum(conv_sum, axis=1)  7.81 us
  transfers between devices with their start and end apart: 9, of which 5 were waited for; matrix products, arithmetic and copies ran while one was open for 17% of the time, Pallas kernels for 0%

commit v1 on v0

--- a/solution.py
+++ b/solution.py
@@ -143,7 +143,7 @@
     ).astype(jnp.bfloat16)
     attn_weight, conv_weight_out = (
         lax.all_gather(out_attn, "sp", axis=1, tiled=True),
-        lax.all_gather(out_conv, "sp", axis=1, tiled=True),
+        jnp.concatenate(lax.all_gather(out_conv, "sp"), axis=1),
     )
     return lax.psum_scatter(
         (

time: 278 us -> 291 us (1.047)
  waiting for transfers between devices: 122 us -> 134 us
  matrix products: 25.7 us -> 19.1 us
  local copies, waits for them, and re-layouts: 12.2 us -> 16.9 us
    all_gather x1, waiting for transfers between devices: 17.5 us -> 26.9 us  [shards(): lax.all_gather(out_conv, 'sp')]
    dot_general x1, matrix products: 7.17 us -> 3.6 us  [shards(): jnp.dot(conv_out, conv_weight_out, preferred_element_type=jnp.float32)]
    dot_general x1, matrix products: 5.72 us -> 2.65 us  [shards(): jnp.dot(attn_out, attn_weight, preferred_element_type=jnp.float32)]
    reduce_scatter x1, waiting for transfers between devices: 43.7 us -> 46.7 us  [shards(): lax.psum_scatter((jnp.dot(attn_out, attn_weight, preferred_element_type=j...]
where the time goes in v1:
time: 291 us; the launch traced here: 290 us
  waiting for transfers between devices  134 us (46%)
  blocking collectives  71.6 us (25%)
  matrix products  19.1 us (7%)
  other arithmetic  18.3 us (6%)
  local copies, waits for them, and re-layouts  16.9 us (6%)
  between operations  13.7 us (5%)
  starting transfers between devices  8.37 us (3%)
  loops' own time  7.57 us (3%)
    reduce_scatter x1, waiting for transfers between devices, shards(): lax.psum_scatter((jnp.dot(attn_out, attn_weight, preferred_element_type=j...  46.7 us
    all_gather x1, waiting for transfers between devices, shards(): lax.all_gather(w_gate, 'sp', axis=0, tiled=True)  41.2 us
    all_gather x1, blocking collectives, shards(): lax.all_gather(w_value, 'sp', axis=0, tiled=True)  34.2 us
    all_gather x1, blocking collectives, shards(): lax.all_gather(w_key, 'sp', axis=0, tiled=True)  31.4 us
    all_gather x1, waiting for transfers between devices, shards(): lax.all_gather(out_conv, 'sp')  26.9 us
    all_gather x1, waiting for transfers between devices, shards(): lax.all_gather(w_content, 'sp', axis=0, tiled=True)  14.7 us
    reduce_sum x1, other arithmetic, shards(): jnp.sum(conv_sum, axis=1)  8.93 us
    ppermute x3, starting transfers between devices, shifted(): return lax.ppermute(block, axis, route)  8.18 us
  transfers between devices with their start and end apart: 9, of which 5 were waited for; matrix products, arithmetic and copies ran while one was open for 17% of the time, Pallas kernels for 0%

profile of v1, /device:TPU:0, one launch (start us, length us, event | category | flops | bytes accessed | tf_op | source)
XLA Modules:
  0.0 289.9 jit_solution(11101624303992550461)
XLA Ops:
  6.5 0.7 all-gather.7.cloned.1.call-update
  7.3 0.0 all-gather.9.cloned.1.call-start
  7.3 0.7 all-gather.9.cloned.1.call-update
  8.0 0.0 all-gather.11.cloned.1.call-start
  8.1 0.7 all-gather.11.cloned.1.call-update
  8.7 0.0 all-gather.15.cloned.1.call-start
  8.8 0.5 all-gather.15.cloned.1.call-update
  9.3 0.0 all-gather.13.cloned.1.call-start
  9.4 0.5 all-gather.13.cloned.1.call-update
  9.9 0.0 reduce-scatter.2.cloned.1.call-start
  10.0 0.5 iota_multiply_fusion
  10.5 1.0 fusion.76
  11.5 1.6 fusion.75
  13.1 3.1 %fusion.20 = f32[1024]{0:T(1024)S(1)} fusion(bf16[1024,2048]{1,0:T(8,128)(2,1)} %param.15), kind=kLoop, calls=%fused_computation.31 | loop fusion | flops 6290432 | bytes 4198400 | tf_op jit(solution)/shard_map/reduce_sum | solution.py:53
  16.2 0.0 copy-start.2
  16.2 0.9 copy.22
  17.1 0.9 copy.23
  18.0 34.2 %all_gather.26 = bf16[2048,64]{1,0:T(8,128)(2,1)S(1)} all-gather(bf16[256,64]{1,0:T(8,128)(2,1)S(1)} %copy.23), channel_id=1, replica_groups=mesh['sp'=8,'tp'=4] {'sp'}, dimensions={0}, use_global_device_ids=true | all-gather | bytes 294912 | tf_op jit(solution)/shard_map/all_gather | solution.py:65
  52.2 31.4 %all_gather.25 = bf16[2048,64]{1,0:T(8,128)(2,1)S(1)} all-gather(bf16[256,64]{1,0:T(8,128)(2,1)S(1)} %copy.22), channel_id=1, replica_groups=mesh['sp'=8,'tp'=4] {'sp'}, dimensions={0}, use_global_device_ids=true | all-gather | bytes 294912 | tf_op jit(solution)/shard_map/all_gather | solution.py:64
  83.6 0.5 multiply_cosine_fusion
  84.1 0.0 all-gather.7.cloned.1.call-done
  84.2 14.7 %all-gather.9.cloned.1.call-done = bf16[2048,256]{1,0:T(8,128)(2,1)} async-done(((bf16[256,256]{1,0:T(8,128)(2,1)}), bf16[2048,256]{1,0:T(8,128)(2,1)}) %all-gather.9.cloned.1.call-update) | async-done | bytes 1048592 | tf_op jit(solution)/shard_map/all_gather | solution.py:66
  98.8 41.2 %all-gather.11.cloned.1.call-done = bf16[2048,256]{1,0:T(8,128)(2,1)} async-done(((bf16[256,256]{1,0:T(8,128)(2,1)}), bf16[2048,256]{1,0:T(8,128)(2,1)}) %all-gather.11.cloned.1.call-update) | async-done | bytes 1048592 | tf_op jit(solution)/shard_map/all_gather | solution.py:67
  140.0 6.7 %concatenate.28 = bf16[2048,896]{1,0:T(8,128)(2,1)} concatenate(bf16[2048,256]{1,0:T(8,128)(2,1)} %all-gather.7.cloned.1.call-done, bf16[2048,64]{1,0:T(8,128)(2,1)S(1)} %all_gather.25, bf16[2048,64]{1,0:T(8,128)(2,1)S(1)} %all_gather.26, bf16[2048,256]{1,0:T(8,128)(2,1)} %all-gather.9.cloned.1.call-done, bf16[2048,256]{1,0:T(8,128)(2,1)} %all-gather.11.cloned.1.call-done), dimensions={1} | concatenate | bytes 7340032 | tf_op jit(solution)/shard_map/concatenate | solution.py:69
  146.7 7.0 %fusion.77 = (bf16[1024,896]{0,1:T(8,128)(2,1)S(1)}, f32[1024,896]{0,1:T(8,128)S(1)}) fusion(f32[1024]{0:T(1024)S(1)} %add_rsqrt_fusion.1, bf16[2048,896]{1,0:T(8,128)(2,1)} %concatenate.28, bf16[1024,2048]{1,0:T(8,128)(2,1)} %param.15, f32[2048]{0:T(1024)S(1)} %copy-done.2), kind=kOutput, calls=%fused_computation.147 | convolution fusion | flops 3766222848 | bytes 13381632 | tf_op jit(solution)/shard_map/dot_general | solution.py:70
  153.7 0.3 fusion.31
  154.1 26.9 %all-gather.15.cloned.1.call-done = bf16[2048,256]{1,0:T(8,128)(2,1)} async-done(((bf16[256,256]{1,0:T(8,128)(2,1)}), bf16[2048,256]{1,0:T(8,128)(2,1)}) %all-gather.15.cloned.1.call-update) | async-done | bytes 1048592 | tf_op jit(solution)/shard_map/all_gather | solution.py:146
  181.0 1.5 copy.25
  182.5 3.1 %collective-permute-start = (bf16[128,1,64]{0,2,1:T(8,128)(2,1)S(1)}, bf16[128,1,64]{0,2,1:T(8,128)(2,1)}, u32[]{:S(2)}, u32[]{:S(2)}) collective-permute-start(bf16[128,1,64]{0,2,1:T(8,128)(2,1)S(1)} %slice_bitcast_fusion.2), channel_id=1, source_target_pairs={{0,4},{4,8},{8,12},{12,16},{16,20},{20,24},{24,28},{1,5},{5,9},{9,... | collective-permute-start | bytes 49160 | tf_op jit(solution)/shard_map/ppermute | solution.py:18
  185.5 0.6 fusion.70
  186.1 2.5 collective-permute-start.1
  188.7 0.1 slice.308
  188.8 2.6 collective-permute-start.2
  191.3 0.1 subtract_convert_fusion
  191.5 1.7 collective-permute-done.2
  193.2 8.9 %fusion.74 = (f32[1024]{0:T(1024)S(1)}, f32[1024]{0:T(1024)S(1)}, f32[1024,256]{0,1:T(8,128)S(1)}) fusion(bf16[1024,256]{0,1:T(8,128)(2,1)S(1)} %get-tuple-element.130, f32[256]{0:T(256)S(1)} %bitcast.121, bf16[30,256]{0,1:T(8,128)(2,1)S(1)} %collective-permute-done.2, f32[256]{0:T(256)S(1)} %bitcast.122, f32[256]{0:T(256)S(1)} %bitcast.124, ...), kind=kLoop, calls=%fused_computation.144 | loop fusion | flops 48756736 | bytes 1629184 | tf_op jit(solution)/shard_map/reduce_sum | solution.py:136
  202.2 6.0 %all-reduce = (f32[1024]{0:T(1024)S(1)}, f32[1024]{0:T(1024)S(1)}) all-reduce(f32[1024]{0:T(1024)S(1)} %get-tuple-element.108, f32[1024]{0:T(1024)S(1)} %get-tuple-element.107), channel_id=1, replica_groups=mesh['sp'=8,'tp'=4] {'tp'}, use_global_device_ids=true, to_apply=%region_8.9 | all-reduce | flops 2048 | bytes 16384 | tf_op jit(solution)/shard_map/psum | solution.py:135
  208.1 0.0 collective-permute-done.1
  208.2 0.0 collective-permute-done
  208.2 0.7 pad_maximum_fusion.2
  208.9 21.1 %while.12 = (s32[]{:T(128)}, bf16[2,512,256]{2,1,0:T(8,128)(2,1)}, s32[2]{0:T(128)}, bf16[1152,1,64]{0,2,1:T(8,128)(2,1)S(1)}, s32[]{:T(128)}, /*index=5*/bf16[1...) while((s32[]{:T(128)}, bf16[2,512,256]{2,1,0:T(8,128)(2,1)}, ...), condition=%wide.region_4.5_spmd, body=%wide.region_1.4_spmd.sunk | while | flops 353048960 | bytes 18868860 | solution.py:129
  208.9 0.0 copy-start
  208.9 1.3 dynamic_slice.46
  214.0 0.4 fusion.91
  214.4 1.2 fusion.92
  215.6 0.1 broadcast_maximum_fusion.2
  215.7 1.1 fusion.93
  216.8 0.1 exponential_add_fusion.2
  216.9 1.7 fusion.94
  218.6 0.1 copy.30
  218.7 0.7 constant_dynamic-update-slice_fusion.2
  219.4 1.3 dynamic_slice.46
  224.5 0.4 fusion.91
  224.9 1.2 fusion.92
  226.1 0.1 broadcast_maximum_fusion.2
  226.2 1.1 fusion.93
  227.3 0.1 exponential_add_fusion.2
  227.4 1.7 fusion.94
  229.1 0.1 copy.30
  229.2 0.7 constant_dynamic-update-slice_fusion.2
  230.0 2.7 fusion.78
  232.6 3.6 %add_convert_fusion = bf16[1024,2048]{1,0:T(8,128)(2,1)} fusion(f32[1024,2048]{1,0:T(8,128)S(1)} %fusion.78, bf16[256,2048]{0,1:T(8,128)(2,1)S(1)} %bitcast.104, f32[1024,256]{0,1:T(8,128)S(1)} %get-tuple-element.127, f32[256]{0:T(256)S(1)} %copy-done.1, f32[1024]{0:T(1024)S(1)} %get-tuple-element.170, f32[1024]{0:T(1024)S(1)} %get-tuple-element.169), kind=kOutput, calls=%fused_computation.32 | convolution fusion | flops 1080033280 | bytes 14689280 | tf_op jit(solution)/shard_map/dot_general | solution.py:151
  236.2 0.0 reduce-scatter.2.cloned.1.call-update
  236.3 46.7 %reduce-scatter.2.cloned.1.call-done = bf16[256,2048]{1,0:T(8,128)(2,1)} async-done(((bf16[1024,2048]{1,0:T(8,128)(2,1)}), bf16[256,2048]{1,0:T(8,128)(2,1)}) %reduce-scatter.2.cloned.1.call-update) | async-done | bytes 1048592 | tf_op jit(solution)/shard_map/reduce_scatter | solution.py:148
  (25 shorter events, 0.2 us)
Async XLA Ops:
  6.5 77.6 %all-gather.7.cloned.1.call-start = ((), (), s32[]{:S(2)}) async-start(), calls=%async_computation.1 | async-start | bytes 1179648 | tf_op jit(solution)/shard_map/all_gather | solution.py:63
  7.3 91.6 %all-gather.9.cloned.1.call-start = ((), (), s32[]{:S(2)}) async-start(), calls=%async_computation.2 | async-start | bytes 1179648 | tf_op jit(solution)/shard_map/all_gather | solution.py:66
  8.0 132.0 %all-gather.11.cloned.1.call-start = ((), (), s32[]{:S(2)}) async-start(), calls=%async_computation.3 | async-start | bytes 1179648 | tf_op jit(solution)/shard_map/all_gather | solution.py:67
  8.7 172.3 %all-gather.15.cloned.1.call-start = ((), (), s32[]{:S(2)}) async-start(), calls=%async_computation.6 | async-start | bytes 1179648 | tf_op jit(solution)/shard_map/all_gather | solution.py:146
  9.3 220.7 %all-gather.13.cloned.1.call-start = ((), (), s32[]{:S(2)}) async-start(), calls=%async_computation.4 | async-start | bytes 1179648 | tf_op jit(solution)/shard_map/all_gather | solution.py:145
  9.9 273.1 %reduce-scatter.2.cloned.1.call-start = ((), (), s32[]{:S(2)}) async-start(), calls=%async_computation.5 | async-start | bytes 5242880 | tf_op jit(solution)/shard_map/reduce_scatter | solution.py:148
  16.2 130.5 %copy-start.2 = (f32[2048]{0:T(1024)S(1)}, f32[2048]{0:T(1024)}, u32[]{:S(2)}) copy-start(f32[2048]{0:T(1024)} %param.16) | copy-start | bytes 24580
  182.5 25.7 %collective-permute-start = (bf16[128,1,64]{0,2,1:T(8,128)(2,1)S(1)}, bf16[128,1,64]{0,2,1:T(8,128)(2,1)}, u32[]{:S(2)}, u32[]{:S(2)}) collective-permute-start(bf16[128,1,64]{0,2,1:T(8,128)(2,1)S(1)} %slice_bitcast_fusion.2), channel_id=1, source_target_pairs={{0,4},{4,8},{8,12},{12,16},{16,20},{20,24},{24,28},{1,5},{5,9},{9,... | collective-permute-start | bytes 49160 | tf_op jit(solution)/shard_map/ppermute | solution.py:18
  186.1 22.0 %collective-permute-start.1 = (bf16[128,1,64]{0,2,1:T(8,128)(2,1)S(1)}, bf16[128,1,64]{0,2,1:T(8,128)(2,1)S(1)}, u32[]{:S(2)}, u32[]{:S(2)}) collective-permute-start(bf16[128,1,64]{0,2,1:T(8,128)(2,1)S(1)} %pad_maximum_fusion.3), channel_id=1, source_target_pairs={{0,4},{4,8},{8,12},{12,16},{16,20},{20,24},{24,28},{1,5},{5,9},{9,... | collective-permute-start | bytes 49160 | tf_op jit(solution)/shard_map/ppermute | solution.py:18
  188.8 4.4 %collective-permute-start.2 = (bf16[30,256]{0,1:T(8,128)(2,1)S(1)}, bf16[30,256]{0,1:T(8,128)(2,1)S(1)}, u32[]{:S(2)}, u32[]{:S(2)}) collective-permute-start(bf16[30,256]{0,1:T(8,128)(2,1)S(1)} %slice.308), channel_id=1, source_target_pairs={{0,4},{4,8},{8,12},{12,16},{16,20},{20,24},{24,28},{1,5},{5,9},{9,... | collective-permute-start | bytes 46088 | tf_op jit(solution)/shard_map/ppermute | solution.py:18
  208.9 6.7 %copy-start = (f32[1,4,1,1]{1,3,2,0:T(1,128)S(1)}, f32[1,4,1,1]{1,3,2,0:T(1,128)}, u32[]{:S(2)}) copy-start(f32[1,4,1,1]{1,3,2,0:T(1,128)} %get-tuple-element.259) | copy-start | bytes 52 | tf_op jit(solution)/shard_map/while
  219.4 6.7 %copy-start = (f32[1,4,1,1]{1,3,2,0:T(1,128)S(1)}, f32[1,4,1,1]{1,3,2,0:T(1,128)}, u32[]{:S(2)}) copy-start(f32[1,4,1,1]{1,3,2,0:T(1,128)} %get-tuple-element.259) | copy-start | bytes 52 | tf_op jit(solution)/shard_map/while
  230.0 2.7 copy-start.1
Sparse Core Ops, SparseCore 0:
  9.5 45.3 all-gather.6
  57.0 41.8 all-gather.8
  101.0 38.9 all-gather.10
  142.0 38.9 all-gather.14
  182.9 38.7 all-gather.12
  236.4 46.5 reduce-scatter.1
